TPU v7x, 256 devices: a 8x8x2 block of a 8x8x16 slice. The times are simulated.
256 devices in a mesh: grp: 2 (over z), fs: 16 (over y, core), tp: 8 (over x).
Axes of the slice: x: 8, y: 8, z: 2, core: 2. Of those that a mesh axis runs over, the one named last changes fastest.
The devices are a block of a 8x8x16 slice.
Arguments:
- prompt_tokens: bfloat16 [32768, 2048], P(('grp', 'fs', 'tp')), parts along dimension 0, may hold values from -6 to 6
- up_weight: float32 [2048, 8192], P('fs', 'tp'), may hold values from -0.125 to 0.125
- down_weight: float32 [2048, 8192], P('fs', 'tp'), may hold values from -0.0625 to 0.0625
- pre_gain: float32 [2048], P('fs'), may hold values from 0.1 to 1.9
- post_gain: float32 [2048], replicated, may hold values from 0.1 to 1.9
Outputs:
- mixed: bfloat16 [32768, 2048], P(('grp', 'fs', 'tp')), parts along dimension 0
- sampler_up: bfloat16 [4096, 8192], P('grp', 'tp'), parts along dimension 0
- sampler_down: bfloat16 [4096, 8192], P('grp', 'tp'), parts along dimension 0
There are 2 independent parts, one for each index of `grp`. A program takes and returns all parts, laid end to end along the dimension named above; an argument that names none is the same for every part. Nothing has to cross between parts.
All inputs are finite; a program needn't handle non-finite values.
Results may differ from a plain program's by a relative error of at most 0.015.
Values may be sent and summed in bfloat16 or wider, within the bound.
A program may use at most 128 MiB of HBM per device.

v0:
```python
import jax
import jax.numpy as jnp
from jax import lax
from jax.sharding import PartitionSpec as P


def sent_together(arrays, axis, dim, along):
    widths = [a.shape[along] for a in arrays]
    both = jnp.concatenate(arrays, axis=along)
    result = lax.all_gather(both, axis, axis=dim, tiled=True)
    return tuple(jnp.split(result, [sum(widths[:k]) for k in range(1, len(widths))], axis=along))


def joined_along(pieces, dim):
    pieces = jnp.moveaxis(pieces, 0, dim)
    dims = pieces.shape
    return pieces.reshape(*dims[:dim], dims[dim] * dims[dim + 1], *dims[dim + 2 :])


def from_everyone(shard, axis):
    size = lax.axis_size(axis)
    return lax.all_to_all(
        jnp.broadcast_to(shard[None], (size, *shard.shape)), axis, 0, 0, tiled=True
    )


def collect(shard, axis, dim):
    return joined_along(from_everyone(shard, axis), dim)


def per_device(prompt_tokens, up_weight, down_weight, pre_gain, post_gain):
    up_local = (up_weight * pre_gain[:, None]).astype(jnp.bfloat16)
    down_local = down_weight.astype(jnp.bfloat16)
    values = prompt_tokens.astype(jnp.float32)
    normed = (values * lax.rsqrt(jnp.mean(values * values, axis=1, keepdims=True) + 1e-06)).astype(
        jnp.bfloat16
    )
    sampler_up, sampler_down = sent_together((up_local, down_local), "fs", 0, 1)
    lifted = jnp.dot(collect(normed, "tp", 0), sampler_up, preferred_element_type=jnp.float32)
    hidden = jnp.square(jax.nn.relu(lifted)).astype(jnp.bfloat16)
    summed = lax.psum_scatter(
        lax.dot_general(
            hidden, sampler_down, (((1,), (1,)), ((), ())), preferred_element_type=jnp.float32
        ).astype(jnp.bfloat16),
        "tp",
        scatter_dimension=0,
        tiled=True,
    ).astype(jnp.float32)
    scaled = summed * lax.rsqrt(jnp.mean(summed * summed, axis=1, keepdims=True) + 1e-06)
    mixed = (scaled * post_gain[None, :]).astype(jnp.bfloat16)
    return (mixed, sampler_up, sampler_down)


def solution(mesh):
    placed = (P(("grp", "fs", "tp"), None), P("fs", "tp"), P("fs", "tp"), P("fs"), P())
    return jax.shard_map(
        per_device,
        mesh=mesh,
        in_specs=placed,
        out_specs=(P(("grp", "fs", "tp"), None), P("grp", "tp"), P("grp", "tp")),
        check_vma=False,
    )
```

profile of v0, /device:TPU:513, one launch (start us, length us, event | category | flops | bytes accessed | tf_op | source)
XLA Modules:
  0.0 213.2 jit_solution(4984359479510517145)
XLA Ops:
  7.2 0.1 all-gather.2.cloned.1.call-start
  7.2 1.1 convert_element_type.27
  8.3 1.1 multiply_convert_fusion.1
  9.5 0.8 pad_maximum_fusion
  10.3 0.1 all-gather.2.cloned.1.call-update
  10.4 1.2 fusion
  11.6 1.2 fusion.1
  12.8 2.5 %broadcast_in_dim.2 = bf16[8,128,2048]{2,1,0:T(8,128)(2,1)} broadcast(bf16[128,2048]{1,0:T(8,128)(2,1)S(1)} %fusion.1), dimensions={1,2} | broadcast | bytes 4718592 | tf_op jit(solution)/shard_map/broadcast_in_dim | solution.py:23
  15.3 7.9 %all-to-all-start = ((bf16[8,128,2048]{2,1,0:T(8,128)(2,1)}), bf16[8,128,2048]{2,1,0:T(8,128)(2,1)}, u32[]{:S(2)}, u32[]{:S(2)}) async-start(bf16[8,128,2048]{2,1,0:T(8,128)(2,1)} %broadcast_in_dim.2), calls=%async_computation | async-start | bytes 8388608 | tf_op jit(solution)/shard_map/all_to_all | solution.py:22
  23.1 0.1 reduce-scatter.2.cloned.1.call-start
  23.2 63.7 %all-gather.2.cloned.1.call-done = bf16[2048,2048]{1,0:T(8,128)(2,1)} async-done(((bf16[128,2048]{1,0:T(8,128)(2,1)}), bf16[2048,2048]{1,0:T(8,128)(2,1)}) %all-gather.2.cloned.1.call-update) | async-done | bytes 8388624 | tf_op jit(solution)/shard_map/all_gather | solution.py:10
  86.9 6.0 %fusion.6 = (bf16[2048,1024]{1,0:T(8,128)(2,1)}, bf16[2048,1024]{1,0:T(8,128)(2,1)}) fusion(bf16[2048,2048]{1,0:T(8,128)(2,1)} %all-gather.2.cloned.1.call-done), kind=kLoop, calls=%fused_computation.16 | loop fusion | bytes 16777216 | tf_op jit(solution)/shard_map/split | solution.py:11
  92.9 14.8 %all-to-all-done = bf16[8,128,2048]{2,1,0:T(8,128)(2,1)} async-done(((bf16[8,128,2048]{2,1,0:T(8,128)(2,1)}), bf16[8,128,2048]{2,1,0:T(8,128)(2,1)}, u32[]{:S(2)}, u32[]{:S(2)}) %all-to-all-start) | async-done | bytes 4194336 | tf_op jit(solution)/shard_map/all_to_all | solution.py:22
  107.7 14.4 %convolution_convert_fusion = bf16[1024,2048]{1,0:T(8,128)(2,1)} fusion(bf16[2048,1024]{1,0:T(8,128)(2,1)} %get-tuple-element.4, bf16[1024,2048]{1,0:T(8,128)(2,1)} %bitcast, bf16[2048,1024]{1,0:T(8,128)(2,1)} %get-tuple-element.3), kind=kOutput, calls=%fused_computation.1 | convolution fusion | flops 8595177472 | bytes 16777216 | tf_op jit(solution)/shard_map/dot_general | solution.py:42
  122.1 0.0 copy-start
  122.1 0.1 reduce-scatter.2.cloned.1.call-update
  122.1 80.9 %reduce-scatter.2.cloned.1.call-done = bf16[128,2048]{1,0:T(8,128)(2,1)} async-done(((bf16[1024,2048]{1,0:T(8,128)(2,1)}), bf16[128,2048]{1,0:T(8,128)(2,1)}) %reduce-scatter.2.cloned.1.call-update) | async-done | bytes 524304 | tf_op jit(solution)/shard_map/reduce_scatter | solution.py:41
  203.1 1.2 fusion.2
  204.3 0.0 copy-done
  204.3 2.0 fusion.4
  (2 shorter events, 0.0 us)
Async XLA Ops:
  7.2 79.7 %all-gather.2.cloned.1.call-start = ((), (), s32[]{:S(2)}) async-start(), calls=%async_computation.2 | async-start | bytes 8912896 | tf_op jit(solution)/shard_map/all_gather | solution.py:10
  15.3 92.4 %all-to-all-start = ((bf16[8,128,2048]{2,1,0:T(8,128)(2,1)}), bf16[8,128,2048]{2,1,0:T(8,128)(2,1)}, u32[]{:S(2)}, u32[]{:S(2)}) async-start(bf16[8,128,2048]{2,1,0:T(8,128)(2,1)} %broadcast_in_dim.2), calls=%async_computation | async-start | bytes 8388608 | tf_op jit(solution)/shard_map/all_to_all | solution.py:22
  23.1 179.9 %reduce-scatter.2.cloned.1.call-start = ((), (), s32[]{:S(2)}) async-start(), calls=%async_computation.3 | async-start | bytes 4718592 | tf_op jit(solution)/shard_map/reduce_scatter | solution.py:41
  122.1 82.2 %copy-start = (f32[2048]{0:T(1024)S(1)}, f32[2048]{0:T(1024)}, u32[]{:S(2)}) copy-start(f32[2048]{0:T(1024)} %param.9) | copy-start | bytes 24580
Sparse Core Ops, SparseCore 0:
  10.5 76.3 all-gather.1
  122.2 80.7 reduce-scatter.1
where the time goes:
time: 214 us; the launch traced here: 213 us
  waiting for transfers between devices  160 us (75%)
  matrix products  14.4 us (7%)
  between operations  14.1 us (7%)
  other arithmetic  8.74 us (4%)
  local copies, waits for them, and re-layouts  8.5 us (4%)
  starting transfers between devices  7.98 us (4%)
    reduce_scatter x1, waiting for transfers between devices, per_device(): lax.psum_scatter(lax.dot_general(hidden, sampler_down, (((1,), (1,)), (()...  80.9 us
    all_gather x1, waiting for transfers between devices, sent_together(): result = lax.all_gather(both, axis, axis=dim, tiled=True)  63.7 us
    all_to_all x1, waiting for transfers between devices, from_everyone(): lax.all_to_all(jnp.broadcast_to(shard[None], (size, *shard.shape)), axis,...  14.8 us
    dot_general x1, matrix products, per_device(): lax.dot_general(hidden, sampler_down, (((1,), (1,)), ((), ())), preferred...  14.4 us
    all_to_all x1, starting transfers between devices, from_everyone(): lax.all_to_all(jnp.broadcast_to(shard[None], (size, *shard.shape)), axis,...  7.86 us
    split x1, local copies, waits for them, and re-layouts, sent_together(): jnp.split(result, [sum(widths[:k]) for k in range(1, len(widths))], axis=...  6.02 us
  transfers between devices with their start and end apart: 3, of which 3 were waited for; matrix products, arithmetic and copies ran while one was open for 5% of the time, Pallas kernels for 0%

commit v1 on v0

v1 whole, which is shorter than its diff:
```python
import functools

import jax
import jax.numpy as jnp
from jax import lax
from jax.experimental import pallas as pl
from jax.experimental.pallas import tpu as pltpu
from jax.sharding import PartitionSpec as P

MESH = pl.DeviceIdType.MESH
EPS = 1e-06
TILE = 256


def ring_items(n):
    far = n // 2
    return [(k % 2, k // 2) for k in range(2 * far - 1)]


def kernel(
    n_tp,
    n_fs,
    tok_hbm,
    up_hbm,
    down_hbm,
    pre_ref,
    post_ref,
    mixed_ref,
    wu,
    wd,
    tok_in,
    up_in,
    down_in,
    tok,
    hid,
    part,
    outbox,
    inbox,
    in_sem,
    x_send,
    x_recv,
    y_send,
    y_recv,
    c_send,
    c_recv,
    r_send,
    r_recv,
):
    t = lax.axis_index("tp")
    f = lax.axis_index("fs")
    x_peer = ({"tp": lax.rem(t + 1, n_tp)}, {"tp": lax.rem(t + n_tp - 1, n_tp)})
    y_peer = ({"fs": lax.rem(f + 2, n_fs)}, {"fs": lax.rem(f + n_fs - 2, n_fs)})
    core_peer = {"fs": f + 1 - 2 * lax.rem(f, 2)}
    rows, width = tok_in.shape
    shard = up_in.shape[0]
    half = rows // 2
    wide = width // 2
    n_pairs = n_tp // 2

    barrier = pltpu.get_barrier_semaphore()
    for peer in (*x_peer, *y_peer, core_peer):
        pl.semaphore_signal(barrier, inc=1, device_id=peer, device_id_type=MESH)
    loads = [
        pltpu.make_async_copy(src, dst, in_sem.at[k])
        for k, (src, dst) in enumerate(((up_hbm, up_in), (down_hbm, down_in), (tok_hbm, tok_in)))
    ]
    for load in loads:
        load.start()

    def shard_rows(index):
        return pl.ds(pl.multiple_of(index * shard, shard), shard)

    loads[0].wait()
    gain = jnp.broadcast_to(pre_ref[...], (shard, shard)).T
    for c in range(up_in.shape[1] // shard):
        cols = pl.ds(c * shard, shard)
        wu[shard_rows(f), cols] = (up_in[:, cols] * gain).astype(jnp.bfloat16)
    loads[1].wait()
    wd[shard_rows(f), :] = down_in[...].astype(jnp.bfloat16)
    loads[2].wait()
    values = tok_in[...].astype(jnp.float32)
    scale = lax.rsqrt(jnp.mean(values * values, axis=1, keepdims=True) + EPS)
    tok[0, rows:, :] = (values * scale).astype(jnp.bfloat16)

    pl.semaphore_wait(barrier, 5)

    def tok_slot(direction, distance):
        if distance == 0:
            return 0, rows
        if distance == n_pairs:
            return 0, 0
        return distance, (rows if direction == 0 else 0)

    def tok_piece(direction, which, distance):
        pair, row = tok_slot(direction, distance)
        return tok.at[pair, pl.ds(row + which * half, half), :]

    def weight_piece(direction, which, distance):
        step = 2 * distance
        owner = lax.rem(f + n_fs - step, n_fs) if direction == 0 else lax.rem(f + step, n_fs)
        return (wu, wd)[which].at[shard_rows(owner), :]

    def x_copy(direction, k):
        which, distance = ring_items(n_tp)[k]
        which = which if direction == 0 else 1 - which
        return pltpu.make_async_remote_copy(
            src_ref=tok_piece(direction, which, distance),
            dst_ref=tok_piece(direction, which, distance + 1),
            send_sem=x_send.at[direction, k],
            recv_sem=x_recv.at[direction, k],
            device_id=x_peer[direction],
            device_id_type=MESH,
        )

    def y_copy(direction, k):
        which, distance = ring_items(n_fs // 2)[k]
        which = which if direction == 0 else 1 - which
        piece = weight_piece(direction, which, distance)
        return pltpu.make_async_remote_copy(
            src_ref=piece,
            dst_ref=piece,
            send_sem=y_send.at[direction, k],
            recv_sem=y_recv.at[direction, k],
            device_id=y_peer[direction],
            device_id_type=MESH,
        )

    def core_copy(slot, piece):
        return pltpu.make_async_remote_copy(
            src_ref=piece,
            dst_ref=piece,
            send_sem=c_send.at[slot],
            recv_sem=c_recv.at[slot],
            device_id=core_peer,
            device_id_type=MESH,
        )

    x_steps = len(ring_items(n_tp))
    y_steps = len(ring_items(n_fs // 2))
    xs = [[x_copy(d, k) for k in range(x_steps)] for d in range(2)]
    ys = [[y_copy(d, k) for k in range(y_steps)] for d in range(2)]
    cs = []
    for k in range(2):
        for d in range(2):
            ys[d][k].start()
        for d in range(2):
            xs[d][k].start()
    for which in range(2):
        cs.append(core_copy(which, weight_piece(0, which, 0)))
        cs[-1].start()
    for k in range(max(x_steps, y_steps)):
        for d in range(2):
            if k < y_steps:
                ys[d][k].wait_recv()
                if k + 2 < y_steps:
                    ys[d][k + 2].start()
                which, distance = ring_items(n_fs // 2)[k]
                which = which if d == 0 else 1 - which
                cs.append(core_copy(2 + d * y_steps + k, weight_piece(d, which, distance + 1)))
                cs[-1].start()
        for d in range(2):
            if k < x_steps:
                xs[d][k].wait_recv()
                if k + 2 < x_steps:
                    xs[d][k + 2].start()
    for copy in cs:
        copy.wait_recv()

    def hidden(pair):
        def one(n, carry):
            cols = pl.ds(pl.multiple_of(n * TILE, TILE), TILE)
            lifted = jnp.dot(tok[pair], wu[:, cols], preferred_element_type=jnp.float32)
            lifted = jnp.maximum(lifted, 0.0)
            hid[pair, :, cols] = (lifted * lifted).astype(jnp.bfloat16)
            return carry

        lax.fori_loop(0, hid.shape[2] // TILE, one, 0)

    def partial(pair, which):
        def one(n, carry):
            cols = pl.ds(pl.multiple_of(which * wide + n * TILE, TILE), TILE)
            part[pair, :, cols] = lax.dot_general(
                hid[pair],
                wd[cols, :],
                (((1,), (1,)), ((), ())),
                preferred_element_type=jnp.float32,
            )
            return carry

        lax.fori_loop(0, wide // TILE, one, 0)

    def r_copy(direction, k):
        return pltpu.make_async_remote_copy(
            src_ref=outbox.at[direction, k],
            dst_ref=inbox.at[direction, k],
            send_sem=r_send.at[direction, k],
            recv_sem=r_recv.at[direction, k],
            device_id=x_peer[direction],
            device_id_type=MESH,
        )

    rs = [[r_copy(d, k) for k in range(x_steps)] for d in range(2)]

    def pass_on(k, directions=(0, 1)):
        for d in directions:
            which, travelled = ring_items(n_tp)[x_steps - 1 - k]
            which = which if d == 0 else 1 - which
            ahead = travelled + 1
            pair, row = (0, 0) if ahead == n_pairs else (ahead, 0 if d == 0 else rows)
            own = part[pair, pl.ds(row, rows), pl.ds(which * wide, wide)]
            if k >= 2:
                rs[d][k - 2].wait_recv()
                own = own + inbox[d, k - 2].astype(jnp.float32)
            outbox[d, k] = own.astype(jnp.bfloat16)
        for d in directions:
            rs[d][k].start()

    hidden(0)
    partial(0, 0)
    pass_on(0, (0,))
    partial(0, 1)
    pass_on(0, (1,))
    for pair in range(n_pairs - 1, 0, -1):
        hidden(pair)
        partial(pair, 0)
        partial(pair, 1)
        first = 2 * (n_pairs - 1 - pair) + 1
        pass_on(first)
        pass_on(first + 1)

    last = x_steps - 1
    halves = []
    for which in range(2):
        total = part[0, pl.ds(rows, rows), pl.ds(which * wide, wide)]
        for d in range(2):
            k = last if which == d else last - 1
            rs[d][k].wait_recv()
            total = total + inbox[d, k].astype(jnp.float32)
        part[0, pl.ds(rows, rows), pl.ds(which * wide, wide)] = total
    total = part[0, pl.ds(rows, rows), :]
    scale = lax.rsqrt(jnp.mean(total * total, axis=1, keepdims=True) + EPS)
    mixed_ref[...] = (total * scale * post_ref[...]).astype(jnp.bfloat16)

    for copies in (*xs, *ys, *rs, cs):
        for copy in copies:
            copy.wait_send()


def solution(mesh):
    n_tp, n_fs = mesh.shape["tp"], mesh.shape["fs"]

    def per_device(prompt_tokens, up_weight, down_weight, pre_gain, post_gain):
        rows, width = prompt_tokens.shape
        shard, units = up_weight.shape
        x_steps, y_steps = len(ring_items(n_tp)), len(ring_items(n_fs // 2))
        vmem = pl.BlockSpec(memory_space=pltpu.VMEM)
        hbm = pl.BlockSpec(memory_space=pl.ANY)
        dma = pltpu.SemaphoreType.DMA
        return pl.pallas_call(
            functools.partial(kernel, n_tp, n_fs),
            out_shape=(
                jax.ShapeDtypeStruct((rows, width), jnp.bfloat16),
                jax.ShapeDtypeStruct((n_fs * shard, units), jnp.bfloat16),
                jax.ShapeDtypeStruct((n_fs * shard, units), jnp.bfloat16),
            ),
            in_specs=[hbm, hbm, hbm, vmem, vmem],
            out_specs=(vmem, vmem, vmem),
            scratch_shapes=[
                pltpu.VMEM((rows, width), jnp.bfloat16),
                pltpu.VMEM((shard, units), jnp.float32),
                pltpu.VMEM((shard, units), jnp.float32),
                pltpu.VMEM((n_tp // 2, 2 * rows, width), jnp.bfloat16),
                pltpu.VMEM((n_tp // 2, 2 * rows, units), jnp.bfloat16),
                pltpu.VMEM((n_tp // 2, 2 * rows, width), jnp.float32),
                pltpu.VMEM((2, x_steps, rows, width // 2), jnp.bfloat16),
                pltpu.VMEM((2, x_steps, rows, width // 2), jnp.bfloat16),
                dma((3,)),
                dma((2, x_steps)),
                dma((2, x_steps)),
                dma((2, y_steps)),
                dma((2, y_steps)),
                dma((2 + 2 * y_steps,)),
                dma((2 + 2 * y_steps,)),
                dma((2, x_steps)),
                dma((2, x_steps)),
            ],
            compiler_params=pltpu.CompilerParams(
                collective_id=0, has_side_effects=True, vmem_limit_bytes=56 * 2**20
            ),
        )(prompt_tokens, up_weight, down_weight, pre_gain[None, :], post_gain[None, :])

    placed = (P(("grp", "fs", "tp"), None), P("fs", "tp"), P("fs", "tp"), P("fs"), P())
    return jax.shard_map(
        per_device,
        mesh=mesh,
        in_specs=placed,
        out_specs=(P(("grp", "fs", "tp"), None), P("grp", "tp"), P("grp", "tp")),
        check_vma=False,
    )
```

time: 214 us -> 120 us (0.56)
  waiting for transfers between devices: 160 us -> 0 us
  Pallas kernels: 0 us -> 110 us
  matrix products: 14.4 us -> 0 us
  between operations: 14.1 us -> 0.64 us
  other arithmetic: 8.74 us -> 0 us
  starting transfers between devices: 7.98 us -> 0 us
    pallas_call x0 -> x1, Pallas kernels: none -> 110 us  [per_device(): pl.pallas_call(functools.partial(kernel, n_tp, n_fs), out_shape=(jax.Shap...]
    reduce_scatter x1 -> x0, waiting for transfers between devices: 80.9 us -> none  [per_device(): lax.psum_scatter(lax.dot_general(hidden, sampler_down, (((1,), (1,)), (()...]
    all_gather x1 -> x0, waiting for transfers between devices: 63.7 us -> none  [sent_together(): result = lax.all_gather(both, axis, axis=dim, tiled=True)]
    all_to_all x1 -> x0, waiting for transfers between devices: 14.8 us -> none  [from_everyone(): lax.all_to_all(jnp.broadcast_to(shard[None], (size, *shard.shape)), axis,...]
    dot_general x1 -> x0, matrix products: 14.4 us -> none  [per_device(): lax.dot_general(hidden, sampler_down, (((1,), (1,)), ((), ())), preferred...]
    unnamed x2 -> x5, local copies, waits for them, and re-layouts: 0.01 us -> 8.71 us
    all_to_all x1 -> x0, starting transfers between devices: 7.86 us -> none  [from_everyone(): lax.all_to_all(jnp.broadcast_to(shard[None], (size, *shard.shape)), axis,...]
    split x1 -> x0, local copies, waits for them, and re-layouts: 6.02 us -> none  [sent_together(): jnp.split(result, [sum(widths[:k]) for k in range(1, len(widths))], axis=...]
  transfers between devices with their start and end apart: 3 -> 0, of which waited for: 3 -> 0; matrix products, arithmetic and copies ran while one was open for 5% -> 0% of each run, Pallas kernels for 0% -> 0%
where the time goes in v1:
time: 120 us; the launch traced here: 119 us
  Pallas kernels  110 us (92%)
  local copies, waits for them, and re-layouts  8.71 us (7%)
    pallas_call x1, Pallas kernels, per_device(): pl.pallas_call(functools.partial(kernel, n_tp, n_fs), out_shape=(jax.Shap...  110 us
    unnamed x5, local copies, waits for them, and re-layouts  8.71 us

profile of v1, /device:TPU:513, one launch (start us, length us, event | category | flops | bytes accessed | tf_op | source)
XLA Modules:
  0.0 119.5 jit_solution(6437113931787805905)
XLA Ops:
  0.6 110.1 %shard_map.76 = (bf16[128,2048]{1,0:T(8,128)(2,1)}, bf16[2048,1024]{1,0:T(8,128)(2,1)}, bf16[2048,1024]{1,0:T(8,128)(2,1)}) custom-call(bf16[128,2048]{1,0:T(8,128)(2,1)} %tok_hbm.1, f32[128,1024]{1,0:T(8,128)} %up_hbm.1, f32[128,1024]{1,0:T(8,128)} %down_hbm.1, f32[1,128]{1,0:T(1,128)} %bitcast.3, f32[1,2048]{1,0:T(1,128)} %bitcast.2), custom_call_target="tpu_custom_call" | custom-call | tf_op jit(solution)/shard_map/pallas_call | solution.py:259
  110.7 1.9 %copy.11 = bf16[128,2048]{1,0:T(8,128)(2,1)} copy(bf16[128,2048]{1,0:T(8,128)(2,1)} %get-tuple-element.6) | data formatting | bytes 1048576
  112.6 0.0 copy-start
  112.6 4.8 %copy.12 = bf16[2048,1024]{1,0:T(8,128)(2,1)} copy(bf16[2048,1024]{1,0:T(8,128)(2,1)} %get-tuple-element.7) | data formatting | bytes 8388608
  117.4 0.0 copy-done
  117.4 2.0 %copy.13 = bf16[2048,1024]{1,0:T(8,128)(2,1)} copy(bf16[2048,1024]{1,0:T(8,128)(2,1)S(1)} %copy-done) | data formatting | bytes 8388608
Async XLA Ops:
  112.6 4.8 %copy-start = (bf16[2048,1024]{1,0:T(8,128)(2,1)S(1)}, bf16[2048,1024]{1,0:T(8,128)(2,1)}, u32[]{:S(2)}) copy-start(bf16[2048,1024]{1,0:T(8,128)(2,1)} %get-tuple-element.8) | copy-start | bytes 12582916

commit v2 on v1

v2 whole, which is shorter than its diff:
```python
import functools

import jax
import jax.numpy as jnp
from jax import lax
from jax.experimental import pallas as pl
from jax.experimental.pallas import tpu as pltpu
from jax.sharding import PartitionSpec as P

MESH = pl.DeviceIdType.MESH
EPS = 1e-06
TILE = 256


def with_hops(chains):
    latest, count, slots = {}, {}, []
    for slot, chain in enumerate(chains):
        slots.append((chain, count.get(chain, 0), latest.get(chain, -1)))
        latest[chain], count[chain] = slot, count.get(chain, 0) + 1
    return slots


def far_first(n):
    far = n // 2
    chains = [c for r in range(far) for c in (0, 1, 2 + r % 2)]
    left = 2 * (far - 1) - far
    return with_hops(chains + [2 + k % 2 for k in range(left)])


def zero_and_two_first(n):
    far = n // 2
    chains = []
    for r in range(far):
        chains += [0] + [2] * (r < far - 1) + [1 if r % 2 == 0 else 3]
    ones, threes = far - chains.count(1), far - 1 - chains.count(3)
    for r in range(ones + threes):
        chains.append(1 if (ones + threes - r) % 2 else 3)
    return with_hops(chains)


def kernel(
    n_tp,
    n_fs,
    tok_hbm,
    up_hbm,
    down_hbm,
    pre_hbm,
    total_ref,
    wu,
    wd,
    tok_in,
    up_in,
    down_in,
    pre_in,
    tok,
    hid,
    part,
    outbox,
    inbox,
    in_sem,
    x_send,
    x_recv,
    y_send,
    y_recv,
    c_send,
    c_recv,
    r_send,
    r_recv,
):
    t = lax.axis_index("tp")
    f = lax.axis_index("fs")
    n_y = n_fs // 2
    y = f // 2
    x_peer = ({"tp": lax.rem(t + 1, n_tp)}, {"tp": lax.rem(t + n_tp - 1, n_tp)})
    y_peer = ({"fs": lax.rem(f + 2, n_fs)}, {"fs": lax.rem(f + n_fs - 2, n_fs)})
    core_peer = {"fs": f + 1 - 2 * lax.rem(f, 2)}
    rows, width = tok_in.shape
    shard = up_in.shape[0]
    strip = rows // 4
    wide = width // 4
    n_pairs = n_tp // 2

    barrier = pltpu.get_barrier_semaphore()
    for peer in (*x_peer, *y_peer, core_peer):
        pl.semaphore_signal(barrier, inc=1, device_id=peer, device_id_type=MESH)
    loads = [
        pltpu.make_async_copy(src, dst, in_sem.at[k])
        for k, (src, dst) in enumerate(((tok_hbm, tok_in), (pre_hbm, pre_in), (up_hbm, up_in), (down_hbm, down_in)))
    ]
    for load in loads:
        load.start()

    def shard_rows(index):
        return pl.ds(pl.multiple_of(index * shard, shard), shard)

    x_slots, y_slots = far_first(n_tp), zero_and_two_first(n_y)

    def tok_strip(direction, chain, distance):
        if distance == 0:
            pair, row = 0, rows
        elif distance == n_pairs:
            pair, row = 0, 0
        else:
            pair, row = distance, (rows if direction == 0 else 0)
        which = chain if direction == 0 else (chain + 2) % 4
        return tok.at[pair, pl.ds(row + which * strip, strip), :]

    def weight_piece(direction, chain, distance):
        step = 2 * distance
        owner = lax.rem(f + n_fs - step, n_fs) if direction == 0 else lax.rem(f + step, n_fs)
        part_of = chain // 2 if direction == 0 else 1 - chain // 2
        piece = pl.ds(pl.multiple_of(owner * shard + part_of * (shard // 2), shard // 2), shard // 2)
        return (wu, wd)[chain % 2].at[piece, :]

    def x_copy(direction, slot):
        chain, hop, _ = x_slots[slot]
        return pltpu.make_async_remote_copy(
            src_ref=tok_strip(direction, chain, hop),
            dst_ref=tok_strip(direction, chain, hop + 1),
            send_sem=x_send.at[direction, slot],
            recv_sem=x_recv.at[direction, slot],
            device_id=x_peer[direction],
            device_id_type=MESH,
        )

    def y_copy(direction, slot):
        chain, hop, _ = y_slots[slot]
        piece = weight_piece(direction, chain, hop)
        return pltpu.make_async_remote_copy(
            src_ref=piece,
            dst_ref=piece,
            send_sem=y_send.at[direction, slot],
            recv_sem=y_recv.at[direction, slot],
            device_id=y_peer[direction],
            device_id_type=MESH,
        )

    def core_copy(slot, piece):
        return pltpu.make_async_remote_copy(
            src_ref=piece,
            dst_ref=piece,
            send_sem=c_send.at[slot],
            recv_sem=c_recv.at[slot],
            device_id=core_peer,
            device_id_type=MESH,
        )

    def r_copy(direction, slot):
        return pltpu.make_async_remote_copy(
            src_ref=outbox.at[direction, slot],
            dst_ref=inbox.at[direction, slot],
            send_sem=r_send.at[direction, slot],
            recv_sem=r_recv.at[direction, slot],
            device_id=x_peer[direction],
            device_id_type=MESH,
        )

    xs = [[x_copy(d, k) for k in range(len(x_slots))] for d in range(2)]
    ys = [[y_copy(d, k) for k in range(len(y_slots))] for d in range(2)]
    rs = [[r_copy(d, k) for k in range(len(x_slots))] for d in range(2)]
    own = [core_copy(which, (wu, wd)[which].at[shard_rows(f), :]) for which in range(2)]
    across = [
        [
            core_copy(2 + d * len(y_slots) + k, weight_piece(d, chain, hop + 1))
            for k, (chain, hop, _) in enumerate(y_slots)
        ]
        for d in range(2)
    ]

    loads[0].wait()
    values = tok_in[...].astype(jnp.float32)
    scale = lax.rsqrt(jnp.mean(values * values, axis=1, keepdims=True) + EPS)
    tok[0, rows:, :] = (values * scale).astype(jnp.bfloat16)
    loads[1].wait()
    loads[2].wait()
    gain = jnp.broadcast_to(pre_in[...], (shard, shard)).T
    for c in range(up_in.shape[1] // shard):
        cols = pl.ds(c * shard, shard)
        wu[shard_rows(f), cols] = (up_in[:, cols] * gain).astype(jnp.bfloat16)

    pl.semaphore_wait(barrier, 5)

    started = {"x": 0, "y": 0}

    def go_on(name, copies, slots, received, limit):
        while started[name] < min(limit, len(slots)) and slots[started[name]][2] <= received:
            for d in range(2):
                copies[d][started[name]].start()
            started[name] += 1

    go_on("x", xs, x_slots, -1, 3)
    go_on("y", ys, y_slots, -1, 2)
    own[0].start()
    loads[3].wait()
    wd[shard_rows(f), :] = down_in[...].astype(jnp.bfloat16)
    go_on("y", ys, y_slots, -1, 3)
    own[1].start()

    settled = [-1]

    def settle(tick):
        if settled[0] == -1:
            own[0].wait_recv()
            own[1].wait_recv()
        for k in range(max(settled[0], 0), tick + 1):
            for d in range(2):
                across[d][k].wait_recv()
        settled[0] = max(settled[0], tick + 1)

    def tick(k):
        if k < len(y_slots):
            for d in range(2):
                ys[d][k].wait_recv()
            go_on("y", ys, y_slots, k, k + 4)
            for d in range(2):
                across[d][k].start()
        if k < len(x_slots):
            for d in range(2):
                xs[d][k].wait_recv()
            go_on("x", xs, x_slots, k, k + 4)

    def hidden(pair):
        def one(n, carry):
            cols = pl.ds(pl.multiple_of(n * TILE, TILE), TILE)
            lifted = jnp.dot(tok[pair], wu[:, cols], preferred_element_type=jnp.float32)
            lifted = jnp.maximum(lifted, 0.0)
            hid[pair, :, cols] = (lifted * lifted).astype(jnp.bfloat16)
            return carry

        lax.fori_loop(0, hid.shape[2] // TILE, one, 0)

    near = n_y // 4
    block = 2 * shard

    def features(quarter, n):
        away = n + (near if quarter >= 2 else 0)
        source = lax.rem(y + away, n_y) if quarter % 2 == 0 else lax.rem(y + n_y - 1 - away, n_y)
        return pl.ds(pl.multiple_of(source * block, block), block)

    def partial(pair, quarter):
        def one(n, carry):
            cols = pl.ds(pl.multiple_of(quarter * wide + n * block, block), block)
            part[pair, :, cols] = lax.dot_general(
                hid[pair],
                wd[features(quarter, n), :],
                (((1,), (1,)), ((), ())),
                preferred_element_type=jnp.float32,
            )
            return carry

        lax.fori_loop(0, near, one, 0)

    def quarter_of(direction, chain):
        return ((0, 2, 1, 3), (1, 3, 0, 2))[direction][chain]

    def ahead(slot):
        chain, hop, _ = x_slots[slot]
        return (n_pairs if chain < 2 else n_pairs - 1) - hop

    def pass_on(slot, directions=(0, 1)):
        chain, hop, before = x_slots[slot]
        steps = ahead(slot)
        for d in directions:
            pair, row = (0, 0) if steps == n_pairs else (steps, 0 if d == 0 else rows)
            mine = part[pair, pl.ds(row, rows), pl.ds(quarter_of(d, chain) * wide, wide)]
            if hop > 0:
                rs[d][before].wait_recv()
                mine = mine + inbox[d, before].astype(jnp.float32)
            outbox[d, slot] = mine.astype(jnp.bfloat16)
        for d in directions:
            rs[d][slot].start()

    last_y = {c: max(k for k, s in enumerate(y_slots) if s[0] == c) for c in range(4)}
    near_y = max(k for k, (c, hop, _) in enumerate(y_slots) if c % 2 == 1 and hop + 1 <= near)
    last_x = max(k for k, s in enumerate(x_slots) if s[0] < 2)
    ready = max(last_x, last_y[0], last_y[2], near_y)
    ticks = max(len(x_slots), len(y_slots))
    begin = min(ready + 1, ticks - 1)
    for k in range(begin + 1):
        tick(k)
    settle(ready)
    hidden(0)
    partial(0, 0)
    partial(0, 1)
    pass_on(0)
    for k in range(begin + 1, ticks):
        tick(k)
    settle(ticks - 2)
    partial(0, 2)
    pass_on(1, (0,))
    settle(ticks - 1)
    partial(0, 3)
    pass_on(1, (1,))

    slots = list(range(2, len(x_slots)))
    for pair in range(n_pairs - 1, 0, -1):
        hidden(pair)
        for quarters in ((0, 1), (2, 3)):
            for quarter in quarters:
                partial(pair, quarter)
            while slots:
                chain = x_slots[slots[0]][0]
                if ahead(slots[0]) < pair:
                    break
                if ahead(slots[0]) == pair and not {quarter_of(d, chain) for d in range(2)} <= set(range(quarters[-1] + 1)):
                    break
                pass_on(slots.pop(0))

    for quarter in (0, 1, 2, 3):
        total = part[0, pl.ds(rows, rows), pl.ds(quarter * wide, wide)]
        for d in range(2):
            slot = max(k for k, s in enumerate(x_slots) if quarter_of(d, s[0]) == quarter)
            rs[d][slot].wait_recv()
            total = total + inbox[d, slot].astype(jnp.float32)
        for n in range(near):
            total_ref[:, features(quarter, n)] = total[:, n * block : (n + 1) * block]

    for copies in (*xs, *ys, *rs, own, *across):
        for copy in copies:
            copy.wait_send()


def finish(total_ref, wu, wd, post_hbm, mixed_hbm, up_hbm, down_hbm, mixed, post, sem):
    load = pltpu.make_async_copy(post_hbm, post, sem.at[3])
    load.start()
    copies = [
        pltpu.make_async_copy(src, dst, sem.at[k])
        for k, (src, dst) in enumerate(((wu, up_hbm), (wd, down_hbm), (mixed, mixed_hbm)))
    ]
    copies[0].start()
    copies[1].start()
    total = total_ref[...]
    scale = lax.rsqrt(jnp.mean(total * total, axis=1, keepdims=True) + EPS)
    load.wait()
    mixed[...] = (total * scale * post[...]).astype(jnp.bfloat16)
    copies[2].start()
    for copy in copies:
        copy.wait()


def solution(mesh):
    n_tp, n_fs = mesh.shape["tp"], mesh.shape["fs"]

    def per_device(*arrays):
        prompt_tokens, up_weight, down_weight, pre_gain, post_gain = (
            pltpu.with_memory_space_constraint(a[None, :] if a.ndim == 1 else a, pltpu.HBM) for a in arrays
        )
        rows, width = prompt_tokens.shape
        shard, units = up_weight.shape
        x_steps, y_steps = len(far_first(n_tp)), len(zero_and_two_first(n_fs // 2))
        vmem = pl.BlockSpec(memory_space=pltpu.VMEM)
        hbm = pl.BlockSpec(memory_space=pltpu.HBM)
        dma = pltpu.SemaphoreType.DMA
        total, sampler_up, sampler_down = pl.pallas_call(
            functools.partial(kernel, n_tp, n_fs),
            out_shape=(
                pltpu.VMEM((rows, width), jnp.float32),
                pltpu.VMEM((n_fs * shard, units), jnp.bfloat16),
                pltpu.VMEM((n_fs * shard, units), jnp.bfloat16),
            ),
            in_specs=[hbm, hbm, hbm, hbm],
            out_specs=(vmem, vmem, vmem),
            scratch_shapes=[
                pltpu.VMEM((rows, width), jnp.bfloat16),
                pltpu.VMEM((shard, units), jnp.float32),
                pltpu.VMEM((shard, units), jnp.float32),
                pltpu.VMEM((1, shard), jnp.float32),
                pltpu.VMEM((n_tp // 2, 2 * rows, width), jnp.bfloat16),
                pltpu.VMEM((n_tp // 2, 2 * rows, units), jnp.bfloat16),
                pltpu.VMEM((n_tp // 2, 2 * rows, width), jnp.float32),
                pltpu.VMEM((2, x_steps, rows, width // 4), jnp.bfloat16),
                pltpu.VMEM((2, x_steps, rows, width // 4), jnp.bfloat16),
                dma((4,)),
                dma((2, x_steps)),
                dma((2, x_steps)),
                dma((2, y_steps)),
                dma((2, y_steps)),
                dma((2 + 2 * y_steps,)),
                dma((2 + 2 * y_steps,)),
                dma((2, x_steps)),
                dma((2, x_steps)),
            ],
            compiler_params=pltpu.CompilerParams(
                collective_id=0, has_side_effects=True, vmem_limit_bytes=42 * 2**20
            ),
        )(prompt_tokens, up_weight, down_weight, pre_gain)
        return pl.pallas_call(
            finish,
            out_shape=(
                jax.ShapeDtypeStruct((rows, width), jnp.bfloat16),
                jax.ShapeDtypeStruct((n_fs * shard, units), jnp.bfloat16),
                jax.ShapeDtypeStruct((n_fs * shard, units), jnp.bfloat16),
            ),
            in_specs=[vmem, vmem, vmem, hbm],
            out_specs=(hbm, hbm, hbm),
            scratch_shapes=[
                pltpu.VMEM((rows, width), jnp.bfloat16),
                pltpu.VMEM((1, width), jnp.float32),
                dma((4,)),
            ],
            compiler_params=pltpu.CompilerParams(vmem_limit_bytes=16 * 2**20),
        )(total, sampler_up, sampler_down, post_gain)

    placed = (P(("grp", "fs", "tp"), None), P("fs", "tp"), P("fs", "tp"), P("fs"), P())
    return jax.shard_map(
        per_device,
        mesh=mesh,
        in_specs=placed,
        out_specs=(P(("grp", "fs", "tp"), None), P("grp", "tp"), P("grp", "tp")),
        check_vma=False,
    )
```

time: 120 us -> 109 us (0.908)
  local copies, waits for them, and re-layouts: 8.71 us -> 0 us
  Pallas kernels: 110 us -> 108 us
    unnamed x5 -> x0, local copies, waits for them, and re-layouts: 8.71 us -> none
    pallas_call x1 -> x2, Pallas kernels: 110 us -> 108 us  [the longest x1 105 us: per_device(): pl.pallas_call(functools.partial(kernel, n_tp, n_fs), out_shape=(pltpu.VM...]
where the time goes in v2:
time: 109 us
  Pallas kernels  108 us (99%)
    pallas_call x1, Pallas kernels, per_device(): pl.pallas_call(functools.partial(kernel, n_tp, n_fs), out_shape=(pltpu.VM...  105 us
    pallas_call x1, Pallas kernels, per_device(): pl.pallas_call(finish, out_shape=(jax.ShapeDtypeStruct((rows, width), jnp...  3.55 us

profile of v2, /device:TPU:513, one launch (start us, length us, event | category | flops | bytes accessed | tf_op | source)
XLA Modules:
  0.0 109.1 jit_solution(11612921429752815120)
XLA Ops:
  0.6 104.9 %shard_map.76 = (f32[128,2048]{1,0:T(8,128)S(1)}, bf16[2048,1024]{1,0:T(8,128)(2,1)S(1)}, bf16[2048,1024]{1,0:T(8,128)(2,1)S(1)}) custom-call(bf16[128,2048]{1,0:T(8,128)(2,1)} %tok_hbm.1, f32[128,1024]{1,0:T(8,128)} %up_hbm.1, f32[128,1024]{1,0:T(8,128)} %down_hbm.1, f32[1,128]{1,0:T(1,128)} %bitcast.3), custom_call_target="tpu_custom_call" | custom-call | tf_op jit(solution)/shard_map/pallas_call | solution.py:354
  105.6 3.6 %shard_map.77 = (bf16[128,2048]{1,0:T(8,128)(2,1)}, bf16[2048,1024]{1,0:T(8,128)(2,1)}, bf16[2048,1024]{1,0:T(8,128)(2,1)}) custom-call(f32[128,2048]{1,0:T(8,128)S(1)} %get-tuple-element.6.total_ref, bf16[2048,1024]{1,0:T(8,128)(2,1)S(1)} %get-tuple-element.7.wu, bf16[2048,1024]{1,0:T(8,128)(2,1)S(1)} %get-tuple-element.8.wd, f32[1,2048]{1,0:T(1,128)} %bitcast.2), custom_call_target="tpu_custom_call" | custom-call | tf_op jit(solution)/shard_map/pallas_call | solution.py:387

commit v3 on v2

--- a/solution.py
+++ b/solution.py
@@ -35,6 +35,18 @@
     ones, threes = far - chains.count(1), far - 1 - chains.count(3)
     for r in range(ones + threes):
         chains.append(1 if (ones + threes - r) % 2 else 3)
+    return with_hops(chains)
+
+
+def near_first(n):
+    far = n // 2
+    chains, left = [0, 2, 0], {0: far - 2, 1: far, 2: far - 2, 3: far - 1}
+    turn = (1, 2, 0, 3)
+    while any(left.values()):
+        for c in turn:
+            if left[c] > 0:
+                chains.append(c)
+                left[c] -= 1
     return with_hops(chains)
 
 
@@ -66,6 +78,7 @@
     c_recv,
     r_send,
     r_recv,
+    here,
 ):
     t = lax.axis_index("tp")
     f = lax.axis_index("fs")
@@ -80,9 +93,18 @@
     wide = width // 4
     n_pairs = n_tp // 2
 
+    core = lax.rem(f, 2)
+    first_row, last_row = y == 0, y == n_y - 1
     barrier = pltpu.get_barrier_semaphore()
-    for peer in (*x_peer, *y_peer, core_peer):
-        pl.semaphore_signal(barrier, inc=1, device_id=peer, device_id_type=MESH)
+
+    def tell(semaphore, peer):
+        pl.semaphore_signal(semaphore, inc=1, device_id=peer, device_id_type=MESH)
+
+    for peer in x_peer:
+        tell(barrier, peer)
+    pl.when(jnp.logical_not(last_row))(lambda: tell(barrier, y_peer[0]))
+    pl.when(first_row)(lambda: tell(barrier, y_peer[1]))
+    pl.when(core == 1)(lambda: tell(barrier, core_peer))
     loads = [
         pltpu.make_async_copy(src, dst, in_sem.at[k])
         for k, (src, dst) in enumerate(((tok_hbm, tok_in), (pre_hbm, pre_in), (up_hbm, up_in), (down_hbm, down_in)))
@@ -93,7 +115,7 @@
     def shard_rows(index):
         return pl.ds(pl.multiple_of(index * shard, shard), shard)
 
-    x_slots, y_slots = far_first(n_tp), zero_and_two_first(n_y)
+    x_slots, y_slots, r_slots = far_first(n_tp), zero_and_two_first(n_y), near_first(n_tp)
 
     def tok_strip(direction, chain, distance):
         if distance == 0:
@@ -171,30 +193,30 @@
     values = tok_in[...].astype(jnp.float32)
     scale = lax.rsqrt(jnp.mean(values * values, axis=1, keepdims=True) + EPS)
     tok[0, rows:, :] = (values * scale).astype(jnp.bfloat16)
+    awaited = 2 + (y > 0).astype(jnp.int32) + last_row.astype(jnp.int32) + (1 - core)
+    pl.semaphore_wait(barrier, awaited)
+    pl.when(y > 0)(lambda: tell(here.at[0], y_peer[1]))
+    pl.when(last_row)(lambda: tell(here.at[1], y_peer[0]))
+    pl.when(core == 0)(lambda: tell(here.at[2], core_peer))
+
+    started = {"x": 0, "y": 0}
+
+    def go_on(name, copies, slots, received, limit):
+        while started[name] < min(limit, len(slots)) and slots[started[name]][2] <= received:
+            for d in range(2):
+                copies[d][started[name]].start()
+            started[name] += 1
+
+    go_on("x", xs, x_slots, -1, 3)
+
     loads[1].wait()
     loads[2].wait()
     gain = jnp.broadcast_to(pre_in[...], (shard, shard)).T
     for c in range(up_in.shape[1] // shard):
         cols = pl.ds(c * shard, shard)
         wu[shard_rows(f), cols] = (up_in[:, cols] * gain).astype(jnp.bfloat16)
-
-    pl.semaphore_wait(barrier, 5)
-
-    started = {"x": 0, "y": 0}
-
-    def go_on(name, copies, slots, received, limit):
-        while started[name] < min(limit, len(slots)) and slots[started[name]][2] <= received:
-            for d in range(2):
-                copies[d][started[name]].start()
-            started[name] += 1
-
-    go_on("x", xs, x_slots, -1, 3)
-    go_on("y", ys, y_slots, -1, 2)
-    own[0].start()
     loads[3].wait()
     wd[shard_rows(f), :] = down_in[...].astype(jnp.bfloat16)
-    go_on("y", ys, y_slots, -1, 3)
-    own[1].start()
 
     settled = [-1]
 
@@ -207,17 +229,31 @@
                 across[d][k].wait_recv()
         settled[0] = max(settled[0], tick + 1)
 
-    def tick(k):
-        if k < len(y_slots):
-            for d in range(2):
-                ys[d][k].wait_recv()
-            go_on("y", ys, y_slots, k, k + 4)
-            for d in range(2):
-                across[d][k].start()
+    def x_tick(k):
         if k < len(x_slots):
             for d in range(2):
                 xs[d][k].wait_recv()
             go_on("x", xs, x_slots, k, k + 4)
+
+    def y_begin():
+        pl.when(jnp.logical_not(last_row))(lambda: pl.semaphore_wait(here.at[0], 1))
+        pl.when(first_row)(lambda: pl.semaphore_wait(here.at[1], 1))
+        go_on("y", ys, y_slots, -1, 3)
+
+    meet = len(y_slots) // 2
+
+    def y_tick(k):
+        for d in range(2):
+            ys[d][k].wait_recv()
+        go_on("y", ys, y_slots, k, k + 4)
+        if k == meet:
+            pl.when(core == 1)(lambda: pl.semaphore_wait(here.at[2], 1))
+            for copy in own:
+                copy.start()
+        if k >= meet:
+            for j in range(0 if k == meet else k, k + 1):
+                for d in range(2):
+                    across[d][j].start()
 
     def hidden(pair):
         def one(n, carry):
@@ -254,11 +290,11 @@
         return ((0, 2, 1, 3), (1, 3, 0, 2))[direction][chain]
 
     def ahead(slot):
-        chain, hop, _ = x_slots[slot]
+        chain, hop, _ = r_slots[slot]
         return (n_pairs if chain < 2 else n_pairs - 1) - hop
 
     def pass_on(slot, directions=(0, 1)):
-        chain, hop, before = x_slots[slot]
+        chain, hop, before = r_slots[slot]
         steps = ahead(slot)
         for d in directions:
             pair, row = (0, 0) if steps == n_pairs else (steps, 0 if d == 0 else rows)
@@ -270,46 +306,68 @@
         for d in directions:
             rs[d][slot].start()
 
-    last_y = {c: max(k for k, s in enumerate(y_slots) if s[0] == c) for c in range(4)}
-    near_y = max(k for k, (c, hop, _) in enumerate(y_slots) if c % 2 == 1 and hop + 1 <= near)
-    last_x = max(k for k, s in enumerate(x_slots) if s[0] < 2)
-    ready = max(last_x, last_y[0], last_y[2], near_y)
-    ticks = max(len(x_slots), len(y_slots))
-    begin = min(ready + 1, ticks - 1)
-    for k in range(begin + 1):
-        tick(k)
-    settle(ready)
-    hidden(0)
-    partial(0, 0)
-    partial(0, 1)
-    pass_on(0)
-    for k in range(begin + 1, ticks):
-        tick(k)
-    settle(ticks - 2)
+    ups = max(k for k, s in enumerate(y_slots) if s[0] % 2 == 0)
+    nears = max(k for k, (c, hop, _) in enumerate(y_slots) if c % 2 == 1 and hop + 1 <= near)
+    nears = max(nears, ups)
+    far_x = max(k for k, s in enumerate(x_slots) if s[0] < 2)
+    last, last_w = len(x_slots) - 1, len(y_slots) - 1
+
+    def first_half(lag):
+        started.update(x=3, y=0)
+        settled[0] = -1
+        done = {"x": 0, "y": 0}
+        y_begin()
+
+        def gather(x_until, y_until):
+            while done["x"] <= x_until or done["y"] <= y_until:
+                if done["x"] <= last and done["x"] <= done["y"] + lag:
+                    x_tick(done["x"])
+                    done["x"] += 1
+                else:
+                    y_tick(done["y"])
+                    done["y"] += 1
+
+        gather(min(far_x + 1, last), min(ups + 1, last_w))
+        settle(ups)
+        hidden(0)
+        gather(min(far_x + 2, last), min(nears + 1, last_w))
+        settle(nears)
+        partial(0, 0)
+        partial(0, 1)
+        pass_on(0)
+        gather(last, min(nears + 1, last_w))
+        hidden(n_pairs - 1)
+        partial(n_pairs - 1, 0)
+        partial(n_pairs - 1, 1)
+        pass_on(1)
+        gather(last, min(nears + 2, last_w))
+        pass_on(2)
+        gather(last, last_w)
+        settle(last_w)
+
+    first_half(1)
+    n_slots = len(x_slots)
     partial(0, 2)
-    pass_on(1, (0,))
-    settle(ticks - 1)
     partial(0, 3)
-    pass_on(1, (1,))
-
-    slots = list(range(2, len(x_slots)))
-    for pair in range(n_pairs - 1, 0, -1):
-        hidden(pair)
-        for quarters in ((0, 1), (2, 3)):
-            for quarter in quarters:
+
+    have = {(0, q) for q in range(4)} | {(n_pairs - 1, q) for q in range(2)}
+    lifted_pairs = {0, n_pairs - 1}
+    for slot in range(3, n_slots):
+        pair = ahead(slot) % n_pairs
+        if pair not in lifted_pairs:
+            hidden(pair)
+            lifted_pairs.add(pair)
+        for d in range(2):
+            quarter = quarter_of(d, r_slots[slot][0])
+            if (pair, quarter) not in have:
                 partial(pair, quarter)
-            while slots:
-                chain = x_slots[slots[0]][0]
-                if ahead(slots[0]) < pair:
-                    break
-                if ahead(slots[0]) == pair and not {quarter_of(d, chain) for d in range(2)} <= set(range(quarters[-1] + 1)):
-                    break
-                pass_on(slots.pop(0))
+                have.add((pair, quarter))
+        pass_on(slot)
 
     for quarter in (0, 1, 2, 3):
         total = part[0, pl.ds(rows, rows), pl.ds(quarter * wide, wide)]
         for d in range(2):
-            slot = max(k for k, s in enumerate(x_slots) if quarter_of(d, s[0]) == quarter)
+            slot = max(k for k, s in enumerate(r_slots) if quarter_of(d, s[0]) == quarter)
             rs[d][slot].wait_recv()
             total = total + inbox[d, slot].astype(jnp.float32)
         for n in range(near):
@@ -379,6 +437,7 @@
                 dma((2 + 2 * y_steps,)),
                 dma((2, x_steps)),
                 dma((2, x_steps)),
+                pltpu.SemaphoreType.REGULAR((3,)),
             ],
             compiler_params=pltpu.CompilerParams(
                 collective_id=0, has_side_effects=True, vmem_limit_bytes=42 * 2**20

time: 109 us -> 107 us (0.982)
  Pallas kernels: 108 us -> 106 us
    pallas_call x1, Pallas kernels: 105 us -> 103 us  [per_device(): pl.pallas_call(functools.partial(kernel, n_tp, n_fs), out_shape=(pltpu.VM...]
where the time goes in v3:
time: 107 us
  Pallas kernels  106 us (99%)
    pallas_call x1, Pallas kernels, per_device(): pl.pallas_call(functools.partial(kernel, n_tp, n_fs), out_shape=(pltpu.VM...  103 us
    pallas_call x1, Pallas kernels, per_device(): pl.pallas_call(finish, out_shape=(jax.ShapeDtypeStruct((rows, width), jnp...  3.55 us

profile of v3, /device:TPU:513, one launch (start us, length us, event | category | flops | bytes accessed | tf_op | source)
XLA Modules:
  0.0 106.8 jit_solution(17132214735072217850)
XLA Ops:
  0.6 102.6 %shard_map.76 = (f32[128,2048]{1,0:T(8,128)S(1)}, bf16[2048,1024]{1,0:T(8,128)(2,1)S(1)}, bf16[2048,1024]{1,0:T(8,128)(2,1)S(1)}) custom-call(bf16[128,2048]{1,0:T(8,128)(2,1)} %tok_hbm.1, f32[128,1024]{1,0:T(8,128)} %up_hbm.1, f32[128,1024]{1,0:T(8,128)} %down_hbm.1, f32[1,128]{1,0:T(1,128)} %bitcast.3), custom_call_target="tpu_custom_call" | custom-call | tf_op jit(solution)/shard_map/pallas_call | solution.py:412
  103.2 3.6 %shard_map.77 = (bf16[128,2048]{1,0:T(8,128)(2,1)}, bf16[2048,1024]{1,0:T(8,128)(2,1)}, bf16[2048,1024]{1,0:T(8,128)(2,1)}) custom-call(f32[128,2048]{1,0:T(8,128)S(1)} %get-tuple-element.6.total_ref, bf16[2048,1024]{1,0:T(8,128)(2,1)S(1)} %get-tuple-element.7.wu, bf16[2048,1024]{1,0:T(8,128)(2,1)S(1)} %get-tuple-element.8.wd, f32[1,2048]{1,0:T(1,128)} %bitcast.2), custom_call_target="tpu_custom_call" | custom-call | tf_op jit(solution)/shard_map/pallas_call | solution.py:446

commit v4 on v3

--- a/solution.py
+++ b/solution.py
@@ -240,20 +240,33 @@
         pl.when(first_row)(lambda: pl.semaphore_wait(here.at[1], 1))
         go_on("y", ys, y_slots, -1, 3)
 
+        @pl.when(core == 0)
+        def _():
+            for copy in own:
+                copy.start()
+
     meet = len(y_slots) // 2
 
     def y_tick(k):
         for d in range(2):
             ys[d][k].wait_recv()
         go_on("y", ys, y_slots, k, k + 4)
-        if k == meet:
-            pl.when(core == 1)(lambda: pl.semaphore_wait(here.at[2], 1))
-            for copy in own:
-                copy.start()
+        @pl.when(core == 0)
+        def _():
+            for d in range(2):
+                across[d][k].start()
+
         if k >= meet:
-            for j in range(0 if k == meet else k, k + 1):
-                for d in range(2):
-                    across[d][j].start()
+
+            @pl.when(core == 1)
+            def _():
+                if k == meet:
+                    pl.semaphore_wait(here.at[2], 1)
+                    for copy in own:
+                        copy.start()
+                for j in range(0 if k == meet else k, k + 1):
+                    for d in range(2):
+                        across[d][j].start()
 
     def hidden(pair):
         def one(n, carry):
@@ -337,9 +350,10 @@
         pass_on(0)
         gather(last, min(nears + 1, last_w))
         hidden(n_pairs - 1)
+        partial(n_pairs - 1, 1)
+        pass_on(1, (0,))
         partial(n_pairs - 1, 0)
-        partial(n_pairs - 1, 1)
-        pass_on(1)
+        pass_on(1, (1,))
         gather(last, min(nears + 2, last_w))
         pass_on(2)
         gather(last, last_w)

time: 107 us -> 107 us (level)
  no operation moved by 1% of the time
where the time goes in v4:
time: 107 us; the launch traced here: 106 us
  Pallas kernels  106 us (99%)
    pallas_call x1, Pallas kernels, per_device(): pl.pallas_call(functools.partial(kernel, n_tp, n_fs), out_shape=(pltpu.VM...  102 us
    pallas_call x1, Pallas kernels, per_device(): pl.pallas_call(finish, out_shape=(jax.ShapeDtypeStruct((rows, width), jnp...  3.55 us

profile of v4, /device:TPU:513, one launch (start us, length us, event | category | flops | bytes accessed | tf_op | source)
XLA Modules:
  0.0 106.4 jit_solution(8723447000711356343)
XLA Ops:
  0.6 102.2 %shard_map.76 = (f32[128,2048]{1,0:T(8,128)S(1)}, bf16[2048,1024]{1,0:T(8,128)(2,1)S(1)}, bf16[2048,1024]{1,0:T(8,128)(2,1)S(1)}) custom-call(bf16[128,2048]{1,0:T(8,128)(2,1)} %tok_hbm.1, f32[128,1024]{1,0:T(8,128)} %up_hbm.1, f32[128,1024]{1,0:T(8,128)} %down_hbm.1, f32[1,128]{1,0:T(1,128)} %bitcast.3), custom_call_target="tpu_custom_call" | custom-call | tf_op jit(solution)/shard_map/pallas_call | solution.py:426
  102.9 3.6 %shard_map.77 = (bf16[128,2048]{1,0:T(8,128)(2,1)}, bf16[2048,1024]{1,0:T(8,128)(2,1)}, bf16[2048,1024]{1,0:T(8,128)(2,1)}) custom-call(f32[128,2048]{1,0:T(8,128)S(1)} %get-tuple-element.6.total_ref, bf16[2048,1024]{1,0:T(8,128)(2,1)S(1)} %get-tuple-element.7.wu, bf16[2048,1024]{1,0:T(8,128)(2,1)S(1)} %get-tuple-element.8.wd, f32[1,2048]{1,0:T(1,128)} %bitcast.2), custom_call_target="tpu_custom_call" | custom-call | tf_op jit(solution)/shard_map/pallas_call | solution.py:460
